TPU v7x, 32 devices: a whole 2x2x4 slice. The times are simulated.
32 devices in a mesh: grp: 2 (over y), fs: 8 (over z, core), tp: 2 (over x).
Axes of the slice: x: 2, y: 2, z: 4, core: 2. Of those that a mesh axis runs over, the one named last changes fastest.
Arguments:
- prompt: bfloat16 [6144, 2048], P(('grp', 'fs')), parts along dimension 0, may hold values from -6 to 6
- routes: int32 [6144, 4], P(('grp', 'fs')), parts along dimension 0, may hold values from 0 to 7, all different within a row; in each aligned block of 384 rows (0 to 383, 384 to 767, ...) at most 240 rows name the same one
- route_weight: float32 [6144, 4], P(('grp', 'fs')), parts along dimension 0, may hold values from 0.2 to 1
- norm_gain: float32 [2048], P('fs'), may hold values from 0.1 to 1.9
- gate_train: float32 [8, 2048, 1024], P(None, 'fs', 'tp'), may hold values from -0.4 to 0.4
- up_train: float32 [8, 2048, 1024], P(None, 'fs', 'tp'), may hold values from -0.4 to 0.4
- down_train: float32 [8, 1024, 2048], P(None, 'fs', 'tp'), may hold values from -0.07 to 0.07
Outputs:
- gate_serve: bfloat16 [16, 2048, 1024], P(('grp', 'fs'), None, 'tp'), parts along dimension 0
- up_serve: bfloat16 [16, 2048, 1024], P(('grp', 'fs'), None, 'tp'), parts along dimension 0
- down_serve: bfloat16 [16, 1024, 2048], P(('grp', 'fs'), 'tp'), parts along dimension 0
- mixed: bfloat16 [6144, 2048], P(('grp', 'fs'), 'tp'), parts along dimension 0
There are 2 independent parts, one for each index of `grp`. A program takes and returns all parts, laid end to end along the dimension named above; an argument that names none is the same for every part. Nothing has to cross between parts.
Inputs may be any that keep to these rules, and one draw needn't show every extreme that they name: `routes`: each row names 4 different experts. Among the rows of one index of fs no expert is named more than 240 times, a bound that some block reaches on some index.
All inputs are finite; a program needn't handle non-finite values.
Results may differ from a plain program's by a relative error of at most 0.012.
Values may be sent and summed in bfloat16 or wider, within the bound.
No kernel may reach another device: no remote copies, remote signals or barrier semaphores. Data moves between devices by JAX's collectives and lax.ppermute only.
A program may use at most 128 MiB of HBM per device.

v0:
```python
import jax
import jax.numpy as jnp
from jax import lax
from jax.sharding import PartitionSpec as P

TOP = 4
LIMIT = 7.0
ALPHA = 1.702
EPS = 1e-06


def shards(prompt, routes, route_weight, norm_gain, gate_train, up_train, down_train):
    gate_cast = (norm_gain[None, :, None] * gate_train).astype(jnp.bfloat16)
    up_cast = (norm_gain[None, :, None] * up_train).astype(jnp.bfloat16)
    down_cast = down_train.astype(jnp.bfloat16)
    gate_mine, up_mine = (
        lax.all_to_all(gate_cast, "fs", split_axis=0, concat_axis=1, tiled=True),
        lax.all_to_all(up_cast, "fs", split_axis=0, concat_axis=1, tiled=True),
    )
    down_rows = lax.all_to_all(down_cast, "fs", split_axis=0, concat_axis=1, tiled=True)
    down_mine = lax.all_to_all(down_rows, "tp", split_axis=1, concat_axis=2, tiled=True)
    tok_rows, width = prompt.shape
    experts = gate_train.shape[0]
    quarter = width // lax.axis_size("tp")
    capacity = min(tok_rows, max(2, 5 * tok_rows * TOP // (4 * experts)))
    values = prompt.astype(jnp.float32)
    normed = (values * lax.rsqrt(jnp.mean(values * values, axis=-1, keepdims=True) + EPS)).astype(
        jnp.bfloat16
    )
    flat_expert = routes.reshape(-1)
    onehot = (flat_expert[:, None] == jnp.arange(experts, dtype=jnp.int32)[None, :]).astype(
        jnp.int32
    )
    earlier = jnp.cumsum(onehot, axis=0) - onehot
    slot_pos = jnp.sum(earlier * onehot, axis=1)
    target = flat_expert * capacity + slot_pos
    source_row = jnp.arange(tok_rows * TOP, dtype=jnp.int32) // TOP
    outbox = jnp.zeros((experts * capacity, width), jnp.bfloat16).at[target].set(normed[source_row])
    inbox = lax.all_to_all(
        outbox.reshape(experts, capacity, width), "fs", split_axis=0, concat_axis=1, tiled=True
    )
    gate_pre = jnp.einsum("erd,edf->erf", inbox, gate_mine, preferred_element_type=jnp.float32)
    up_pre = jnp.einsum("erd,edf->erf", inbox, up_mine, preferred_element_type=jnp.float32)
    gate_pre = jnp.minimum(gate_pre, LIMIT)
    up_pre = jnp.clip(up_pre, -LIMIT, LIMIT)
    hidden = ((up_pre + 1.0) * gate_pre * jax.nn.sigmoid(ALPHA * gate_pre)).astype(jnp.bfloat16)
    own_width = hidden.shape[2]
    empty = jnp.zeros((hidden.shape[0], hidden.shape[1], down_rows.shape[2]), jnp.float32)
    total = empty
    piece = lax.all_gather(hidden, "tp", axis=2, tiled=True)
    for index in range(piece.shape[2] // own_width):
        cols = piece[:, :, index * own_width : (index + 1) * own_width]
        weight_rows = lax.dynamic_slice_in_dim(down_rows, index * own_width, own_width, 1)
        part = jnp.einsum(
            "erf,efd->erd", cols, weight_rows, preferred_element_type=jnp.float32
        ).astype(jnp.bfloat16)
        total = total + part.astype(jnp.float32)
    summed = total.astype(jnp.bfloat16)
    back = lax.all_to_all(summed, "fs", split_axis=1, concat_axis=0, tiled=True)
    picked = back.reshape(experts * capacity, quarter)[target].astype(jnp.float32)
    weighted = picked.reshape(tok_rows, TOP, quarter) * route_weight[:, :, None]
    mixed = jnp.sum(weighted, axis=1).astype(jnp.bfloat16)
    return (gate_mine, up_mine, down_mine, mixed)


def solution(mesh):
    return jax.shard_map(
        shards,
        mesh=mesh,
        in_specs=(
            P(("grp", "fs"), None),
            P(("grp", "fs"), None),
            P(("grp", "fs"), None),
            P("fs"),
            P(None, "fs", "tp"),
            P(None, "fs", "tp"),
            P(None, "fs", "tp"),
        ),
        out_specs=(
            P(("grp", "fs"), None, "tp"),
            P(("grp", "fs"), None, "tp"),
            P(("grp", "fs"), "tp", None),
            P(("grp", "fs"), "tp"),
        ),
        check_vma=False,
    )
```

profile of v0, /device:TPU:0, one launch (start us, length us, event | category | flops | bytes accessed | tf_op | source)
XLA Modules:
  0.0 601.2 jit_solution(9907944391653193153)
XLA Ops:
  7.2 6.8 %multiply_convert_fusion = (bf16[8,256,512]{2,1,0:T(8,128)(2,1)}, bf16[8,256,512]{2,1,0:T(8,128)(2,1)}) fusion(f32[8,256,512]{2,1,0:T(8,128)} %param.12, f32[256]{0:T(256)} %param.10, f32[8,256,512]{2,1,0:T(8,128)} %param.11), kind=kLoop, calls=%fused_computation.7 | loop fusion | flops 4194304 | bytes 12583936 | tf_op jit(solution)/shard_map/convert_element_type | solution.py:14
  14.0 6.5 %all-to-all-start = ((bf16[8,256,512]{2,1,0:T(8,128)(2,1)}), bf16[8,256,512]{2,1,0:T(8,128)(2,1)S(1)}, u32[]{:S(2)}, u32[]{:S(2)}) async-start(bf16[8,256,512]{2,1,0:T(8,128)(2,1)} %get-tuple-element.17), calls=%async_computation | async-start | bytes 4194304 | tf_op jit(solution)/shard_map/all_to_all | solution.py:17
  29.4 33.0 %scatter_custom_fusion = bf16[1920,2048]{1,0:T(8,128)(2,1)} fusion(s32[1536]{0:T(1024)S(1)} %fusion.11, bf16[384,2048]{1,0:T(8,128)(2,1)} %fusion.5, s32[2048]{0:T(1024)S(1)} %pad_clamp_fusion.1, bf16[]{:T(256)} %constant.17.clone.1), kind=kCustom, calls=%fused_computation.4 | custom fusion | bytes 7864832 | tf_op jit(solution)/shard_map/scatter | solution.py:38
  62.4 7.1 %all-to-all-done = bf16[8,256,512]{2,1,0:T(8,128)(2,1)S(1)} async-done(((bf16[8,256,512]{2,1,0:T(8,128)(2,1)}), bf16[8,256,512]{2,1,0:T(8,128)(2,1)S(1)}, u32[]{:S(2)}, u32[]{:S(2)}) %all-to-all-start) | async-done | bytes 2097184 | tf_op jit(solution)/shard_map/all_to_all | solution.py:17
  69.5 178.2 %all_to_all.72 = bf16[8,240,2048]{2,1,0:T(8,128)(2,1)} all-to-all(bf16[8,240,2048]{2,1,0:T(8,128)(2,1)} %bitcast.61), channel_id=1, replica_groups=mesh['grp'=2,'fs'=8,'tp'=2] {'fs'}, dimensions={0} | all-to-all | bytes 15728640 | tf_op jit(solution)/shard_map/all_to_all | solution.py:39
  247.7 4.4 all-to-all-start.1
  252.1 9.5 %fusion.13 = f32[1920,512]{1,0:T(8,128)} fusion(bf16[1920,2048]{1,0:T(8,128)(2,1)} %bitcast.73, bf16[2048,512]{1,0:T(8,128)(2,1)S(1)} %bitcast.70), kind=kOutput, calls=%fused_computation.45 | convolution fusion | flops 4026531840 | bytes 13893632 | tf_op jit(solution)/shard_map/erd,edf->erf/dot_general | solution.py:42
  261.6 39.5 %all-to-all-done.1 = bf16[8,256,512]{2,1,0:T(8,128)(2,1)} async-done(((bf16[8,256,512]{2,1,0:T(8,128)(2,1)}), bf16[8,256,512]{2,1,0:T(8,128)(2,1)}, u32[]{:S(2)}, u32[]{:S(2)}) %all-to-all-start.1) | async-done | bytes 2097184 | tf_op jit(solution)/shard_map/all_to_all | solution.py:18
  301.1 11.8 %multiply_convert_fusion.2 = bf16[1920,512]{1,0:T(8,128)(2,1)} fusion(f32[1920,512]{1,0:T(8,128)} %fusion.13, bf16[1920,2048]{1,0:T(8,128)(2,1)} %bitcast.74, bf16[2048,512]{1,0:T(8,128)(2,1)} %bitcast.8), kind=kOutput, calls=%fused_computation.11 | convolution fusion | flops 4036362240 | bytes 15859712 | tf_op jit(solution)/shard_map/erd,edf->erf/dot_general | solution.py:43
  315.4 51.7 %all_to_all.73 = bf16[8,128,1024]{2,1,0:T(8,128)(2,1)S(1)} all-to-all(bf16[8,128,1024]{2,1,0:T(8,128)(2,1)S(1)} %convert_element_type.62), channel_id=1, replica_groups=mesh['grp'=2,'fs'=8,'tp'=2] {'fs'}, dimensions={0} | all-to-all | bytes 4194304 | tf_op jit(solution)/shard_map/all_to_all | solution.py:20
  368.4 5.2 copy.46
  374.1 12.8 %reduce.6 = bf16[1024,1024]{1,0:T(8,128)(2,1)S(1)} reduce(bf16[1024,1,1024]{2,1,0:T(2,128)(2,1)} %bitcast.64, bf16[]{:T(256)} %broadcast.146), dimensions={1}, to_apply=%bitcast.58.reduce_sub_computation | reduce | bytes 4194306
  389.4 4.2 all-to-all-start.3
  393.6 4.2 fusion.6
  400.1 27.0 %copy.45 = bf16[1,1920,1024]{2,0,1:T(2,128)(2,1)} copy(bf16[1,1920,1024]{2,1,0:T(8,128)(2,1)S(1)} %fusion.2) | data formatting | bytes 7864320 | tf_op jit(solution)/shard_map/convert_element_type | solution.py:58
  427.1 24.6 %reduce.7 = bf16[1920,1024]{1,0:T(8,128)(2,1)} reduce(bf16[1920,1,1024]{2,1,0:T(2,128)(2,1)} %bitcast.62, bf16[]{:T(256)} %broadcast.146), dimensions={1}, to_apply=%bitcast.57.reduce_sub_computation | reduce | bytes 7864322
  451.7 7.6 %reshape.225 = bf16[8,2,122880]{2,1,0:T(2,128)(2,1)} reshape(bf16[1920,1024]{1,0:T(8,128)(2,1)} %reduce.7) | data formatting | bytes 7864320
  459.3 4.8 all-to-all-start.5
  476.9 75.6 %all-to-all-done.5 = bf16[8,2,122880]{2,1,0:T(2,128)(2,1)} async-done(((bf16[8,2,122880]{2,1,0:T(2,128)(2,1)}), bf16[8,2,122880]{2,1,0:T(2,128)(2,1)}, u32[]{:S(2)}, u32[]{:S(2)}) %all-to-all-start.5) | async-done | bytes 3932192 | tf_op jit(solution)/shard_map/all_to_all | solution.py:59
  552.5 8.5 %reshape.226 = bf16[1920,1,1024]{2,1,0:T(2,128)(2,1)} reshape(bf16[8,2,122880]{2,1,0:T(2,128)(2,1)} %all-to-all-done.5) | data formatting | bytes 7864320
  561.0 6.8 %copy.44 = bf16[1,1920,1024]{2,1,0:T(8,128)(2,1)} copy(bf16[1,1920,1024]{2,0,1:T(2,128)(2,1)} %bitcast.63) | data formatting | bytes 7864320
  567.8 9.7 %gather_fusion = bf16[1536,1024]{1,0:T(8,128)(2,1)S(1)} fusion(bf16[1920,1024]{1,0:T(8,128)(2,1)} %bitcast.60, s32[2048]{0:T(1024)S(1)} %pad_clamp_fusion), kind=kCustom, calls=%fused_computation.1 | custom fusion | bytes 6297600 | tf_op jit(solution)/shard_map/gather | solution.py:60
  577.5 4.4 reshape.190
  581.9 7.9 %multiply_reduce_fusion = bf16[384,1024]{1,0:T(8,128)(2,1)} fusion(f32[384,4,1024]{2,1,0:T(4,128)} %reshape.190, f32[384,4]{1,0:T(8,128)S(1)} %copy.35), kind=kLoop, calls=%fused_computation.6 | loop fusion | flops 2752512 | bytes 7084032 | tf_op jit(solution)/shard_map/reduce_sum | solution.py:62
  (48 shorter events, 35.2 us)
Async XLA Ops:
  14.0 6.5 %copy-start.4 = (s32[384,4]{0,1:T(4,128)S(1)}, s32[384,4]{0,1:T(4,128)}, u32[]{:S(2)}) copy-start(s32[384,4]{0,1:T(4,128)} %param.8) | copy-start | bytes 18436
  14.0 55.5 %all-to-all-start = ((bf16[8,256,512]{2,1,0:T(8,128)(2,1)}), bf16[8,256,512]{2,1,0:T(8,128)(2,1)S(1)}, u32[]{:S(2)}, u32[]{:S(2)}) async-start(bf16[8,256,512]{2,1,0:T(8,128)(2,1)} %get-tuple-element.17), calls=%async_computation | async-start | bytes 4194304 | tf_op jit(solution)/shard_map/all_to_all | solution.py:17
  69.5 182.6 %copy-start.2 = (bf16[8,256,512]{2,1,0:T(8,128)(2,1)}, bf16[8,256,512]{2,1,0:T(8,128)(2,1)S(1)}, u32[]{:S(2)}) copy-start(bf16[8,256,512]{2,1,0:T(8,128)(2,1)S(1)} %all-to-all-done) | copy-start | bytes 6291460
  247.7 53.4 %all-to-all-start.1 = ((bf16[8,256,512]{2,1,0:T(8,128)(2,1)}), bf16[8,256,512]{2,1,0:T(8,128)(2,1)}, u32[]{:S(2)}, u32[]{:S(2)}) async-start(bf16[8,256,512]{2,1,0:T(8,128)(2,1)} %get-tuple-element.16), calls=%async_computation.1 | async-start | bytes 4194304 | tf_op jit(solution)/shard_map/all_to_all | solution.py:18
  252.1 141.5 %all-gather.3.cloned.1.call-start = ((), (), s32[]{:S(2)}) async-start(), calls=%async_computation.6 | async-start | bytes 5898240 | tf_op jit(solution)/shard_map/all_gather | solution.py:50
  367.1 1.3 copy-start
  389.4 69.9 %all-to-all-start.3 = ((bf16[2,2,262144]{2,1,0:T(2,128)(2,1)}), bf16[2,2,262144]{2,1,0:T(2,128)(2,1)S(1)}, u32[]{:S(2)}, u32[]{:S(2)}) async-start(bf16[2,2,262144]{2,1,0:T(2,128)(2,1)} %reshape.227), calls=%async_computation.3 | async-start | bytes 4194304 | tf_op jit(solution)/shard_map/all_to_all | solution.py:21
  393.6 4.2 copy-start.1
  393.6 4.2 copy-start.6
  459.3 4.9 copy-start.5
  459.3 93.2 %all-to-all-start.5 = ((bf16[8,2,122880]{2,1,0:T(2,128)(2,1)}), bf16[8,2,122880]{2,1,0:T(2,128)(2,1)}, u32[]{:S(2)}, u32[]{:S(2)}) async-start(bf16[8,2,122880]{2,1,0:T(2,128)(2,1)} %reshape.225), calls=%async_computation.5 | async-start | bytes 7864320 | tf_op jit(solution)/shard_map/all_to_all | solution.py:59
  581.9 7.9 %copy-start.3 = (bf16[8,256,512]{2,1,0:T(8,128)(2,1)S(1)}, bf16[8,256,512]{2,1,0:T(8,128)(2,1)}, u32[]{:S(2)}) copy-start(bf16[8,256,512]{2,1,0:T(8,128)(2,1)} %copy-done.2) | copy-start | bytes 6291460
Sparse Core Ops, SparseCore 0:
  313.0 52.6 all-gather.2
where the time goes:
time: 605 us; the launch traced here: 601 us
  blocking collectives  230 us (38%)
  local copies, waits for them, and re-layouts  125 us (21%)
  waiting for transfers between devices  122 us (20%)
  other arithmetic  62.4 us (10%)
  matrix products  27.7 us (5%)
  starting transfers between devices  19.9 us (3%)
  between operations  14.4 us (2%)
    all_to_all x1, blocking collectives, shards(): lax.all_to_all(outbox.reshape(experts, capacity, width), 'fs', split_axis...  178 us
    all_to_all x1, waiting for transfers between devices, shards(): back = lax.all_to_all(summed, 'fs', split_axis=1, concat_axis=0, tiled=True)  75.6 us
    all_to_all x1, blocking collectives, shards(): lax.all_to_all(down_cast, 'fs', split_axis=0, concat_axis=1, tiled=True)  51.7 us
    unnamed x26, local copies, waits for them, and re-layouts  41.9 us
    all_to_all x1, waiting for transfers between devices, shards(): lax.all_to_all(up_cast, 'fs', split_axis=0, concat_axis=1, tiled=True)  39.5 us
    unnamed x3, other arithmetic  37.4 us
    scatter x1, local copies, waits for them, and re-layouts, shards(): jnp.zeros((experts * capacity, width), jnp.bfloat16).at[target]  33 us
    convert_element_type x1, local copies, waits for them, and re-layouts, shards(): summed = total.astype(jnp.bfloat16)  27 us
  transfers between devices with their start and end apart: 5, of which 3 were waited for; matrix products, arithmetic and copies ran while one was open for 25% of the time, Pallas kernels for 0%

commit v1 on v0

--- a/solution.py
+++ b/solution.py
@@ -7,6 +7,28 @@
 LIMIT = 7.0
 ALPHA = 1.702
 EPS = 1e-06
+
+
+def in_blocks(array, dim, devices):
+    before, after = (array.shape[:dim], array.shape[dim + 1 :])
+    return jnp.moveaxis(array.reshape(*before, devices, -1, *after), dim, 0)
+
+
+def joined_along(blocks, dim):
+    blocks = jnp.moveaxis(blocks, 0, dim)
+    shape = blocks.shape
+    return blocks.reshape(*shape[:dim], shape[dim] * shape[dim + 1], *shape[dim + 2 :])
+
+
+def exchange_in_pairs(x, axis, split_dim, concat_dim):
+    devices, position = (lax.axis_size(axis), lax.axis_index(axis))
+    blocks = in_blocks(x, split_dim, devices)
+    finished = [blocks[position]]
+    for step in range(1, devices):
+        sent = blocks[position ^ step]
+        finished.append(lax.ppermute(sent, axis, [(i, i ^ step) for i in range(devices)]))
+    blocks = jnp.stack(finished)[position ^ jnp.arange(devices)]
+    return joined_along(blocks, concat_dim)
 
 
 def shards(prompt, routes, route_weight, norm_gain, gate_train, up_train, down_train):
@@ -56,7 +78,7 @@
         ).astype(jnp.bfloat16)
         total = total + part.astype(jnp.float32)
     summed = total.astype(jnp.bfloat16)
-    back = lax.all_to_all(summed, "fs", split_axis=1, concat_axis=0, tiled=True)
+    back = exchange_in_pairs(summed, "fs", 1, 0)
     picked = back.reshape(experts * capacity, quarter)[target].astype(jnp.float32)
     weighted = picked.reshape(tok_rows, TOP, quarter) * route_weight[:, :, None]
     mixed = jnp.sum(weighted, axis=1).astype(jnp.bfloat16)

time: 605 us -> 565 us (0.934)
  the two profiles are of different devices: /device:TPU:0 before, /device:TPU:9 now
where the time goes in v1:
time: 565 us; the launch traced here: 561 us
  blocking collectives  179 us (32%)
  waiting for transfers between devices  172 us (30%)
  local copies, waits for them, and re-layouts  90.7 us (16%)
  other arithmetic  40.3 us (7%)
  starting transfers between devices  37.1 us (7%)
  matrix products  27.3 us (5%)
  between operations  14.5 us (3%)
    all_to_all x1, blocking collectives, shards(): lax.all_to_all(outbox.reshape(experts, capacity, width), 'fs', split_axis...  179 us
    ppermute x7, waiting for transfers between devices, exchange_in_pairs(): lax.ppermute(sent, axis, [(i, i ^ step) for i in range(devices)])  74.5 us
    all_to_all x1, waiting for transfers between devices, shards(): lax.all_to_all(down_cast, 'fs', split_axis=0, concat_axis=1, tiled=True)  45.4 us
    all_to_all x1, waiting for transfers between devices, shards(): lax.all_to_all(up_cast, 'fs', split_axis=0, concat_axis=1, tiled=True)  36 us
    scatter x1, local copies, waits for them, and re-layouts, shards(): jnp.zeros((experts * capacity, width), jnp.bfloat16).at[target]  33.3 us
    unnamed x31, local copies, waits for them, and re-layouts  27.4 us
    unnamed x2, other arithmetic  14.2 us
    all_to_all x1, waiting for transfers between devices, shards(): lax.all_to_all(down_rows, 'tp', split_axis=1, concat_axis=2, tiled=True)  12.8 us
  transfers between devices with their start and end apart: 12, of which 9 were waited for; matrix products, arithmetic and copies ran while one was open for 19% of the time, Pallas kernels for 0%

profile of v1, /device:TPU:9, one launch (start us, length us, event | category | flops | bytes accessed | tf_op | source)
XLA Modules:
  0.0 560.9 jit_solution(3749550151107031715)
XLA Ops:
  7.2 6.8 %multiply_convert_fusion = (bf16[8,256,512]{2,1,0:T(8,128)(2,1)}, bf16[8,256,512]{2,1,0:T(8,128)(2,1)}) fusion(f32[8,256,512]{2,1,0:T(8,128)} %param.12, f32[256]{0:T(256)} %param.10, f32[8,256,512]{2,1,0:T(8,128)} %param.11), kind=kLoop, calls=%fused_computation.8 | loop fusion | flops 4194304 | bytes 12583936 | tf_op jit(solution)/shard_map/convert_element_type | solution.py:36
  14.0 5.7 %all-to-all-start = ((bf16[8,256,512]{2,1,0:T(8,128)(2,1)}), bf16[8,256,512]{2,1,0:T(8,128)(2,1)S(1)}, u32[]{:S(2)}, u32[]{:S(2)}) async-start(bf16[8,256,512]{2,1,0:T(8,128)(2,1)} %get-tuple-element.25), calls=%async_computation | async-start | bytes 4194304 | tf_op jit(solution)/shard_map/all_to_all | solution.py:39
  28.4 33.3 %scatter_custom_fusion = bf16[1920,2048]{1,0:T(8,128)(2,1)} fusion(s32[1536]{0:T(1024)S(1)} %fusion.10, bf16[384,2048]{1,0:T(8,128)(2,1)} %fusion.4, s32[2048]{0:T(1024)S(1)} %pad_clamp_fusion.1, bf16[]{:T(256)} %constant.24.clone.1), kind=kCustom, calls=%fused_computation.5 | custom fusion | bytes 7864832 | tf_op jit(solution)/shard_map/scatter | solution.py:60
  65.3 178.7 %all_to_all.63 = bf16[8,240,2048]{2,1,0:T(8,128)(2,1)} all-to-all(bf16[8,240,2048]{2,1,0:T(8,128)(2,1)} %bitcast.85), channel_id=1, replica_groups=mesh['grp'=2,'fs'=8,'tp'=2] {'fs'}, dimensions={0} | all-to-all | bytes 15728640 | tf_op jit(solution)/shard_map/all_to_all | solution.py:61
  244.0 7.2 %all-to-all-start.1 = ((bf16[8,256,512]{2,1,0:T(8,128)(2,1)}), bf16[8,256,512]{2,1,0:T(8,128)(2,1)}, u32[]{:S(2)}, u32[]{:S(2)}) async-start(bf16[8,256,512]{2,1,0:T(8,128)(2,1)} %get-tuple-element.24), calls=%async_computation.1 | async-start | bytes 4194304 | tf_op jit(solution)/shard_map/all_to_all | solution.py:40
  251.2 9.5 %fusion.13 = f32[1920,512]{1,0:T(8,128)} fusion(bf16[1920,2048]{1,0:T(8,128)(2,1)} %bitcast.95, bf16[2048,512]{1,0:T(8,128)(2,1)S(1)} %bitcast.92), kind=kOutput, calls=%fused_computation.61 | convolution fusion | flops 4026531840 | bytes 13893632 | tf_op jit(solution)/shard_map/erd,edf->erf/dot_general | solution.py:64
  260.7 36.0 %all-to-all-done.1 = bf16[8,256,512]{2,1,0:T(8,128)(2,1)} async-done(((bf16[8,256,512]{2,1,0:T(8,128)(2,1)}), bf16[8,256,512]{2,1,0:T(8,128)(2,1)}, u32[]{:S(2)}, u32[]{:S(2)}) %all-to-all-start.1) | async-done | bytes 2097184 | tf_op jit(solution)/shard_map/all_to_all | solution.py:40
  296.7 11.6 %multiply_convert_fusion.2 = bf16[1920,512]{1,0:T(8,128)(2,1)} fusion(f32[1920,512]{1,0:T(8,128)} %fusion.13, bf16[1920,2048]{1,0:T(8,128)(2,1)} %bitcast.96, bf16[2048,512]{1,0:T(8,128)(2,1)} %bitcast.8), kind=kOutput, calls=%fused_computation.10 | convolution fusion | flops 4036362240 | bytes 15859712 | tf_op jit(solution)/shard_map/erd,edf->erf/dot_general | solution.py:65
  312.2 7.4 %all-to-all-start.2 = ((bf16[8,128,1024]{2,1,0:T(8,128)(2,1)}), bf16[8,128,1024]{2,1,0:T(8,128)(2,1)S(1)}, u32[]{:S(2)}, u32[]{:S(2)}) async-start(bf16[8,128,1024]{2,1,0:T(8,128)(2,1)} %convert_element_type.60), calls=%async_computation.2 | async-start | bytes 4194304 | tf_op jit(solution)/shard_map/all_to_all | solution.py:42
  319.7 45.4 %all-to-all-done.2 = bf16[8,128,1024]{2,1,0:T(8,128)(2,1)S(1)} async-done(((bf16[8,128,1024]{2,1,0:T(8,128)(2,1)}), bf16[8,128,1024]{2,1,0:T(8,128)(2,1)S(1)}, u32[]{:S(2)}, u32[]{:S(2)}) %all-to-all-start.2) | async-done | bytes 2097184 | tf_op jit(solution)/shard_map/all_to_all | solution.py:42
  365.1 5.2 copy.39
  370.8 14.1 %reduce.6 = bf16[1024,1024]{1,0:T(8,128)(2,1)} reduce(bf16[1024,1,1024]{2,1,0:T(2,128)(2,1)} %bitcast.86, bf16[]{:T(256)} %broadcast.185), dimensions={1}, to_apply=%bitcast.82.reduce_sub_computation | reduce | bytes 4194306
  388.6 4.9 all-to-all-start.3
  405.3 12.8 %all-to-all-done.3 = bf16[2,2,262144]{2,1,0:T(2,128)(2,1)} async-done(((bf16[2,2,262144]{2,1,0:T(2,128)(2,1)}), bf16[2,2,262144]{2,1,0:T(2,128)(2,1)}, u32[]{:S(2)}, u32[]{:S(2)}) %all-to-all-start.3) | async-done | bytes 2097184 | tf_op jit(solution)/shard_map/all_to_all | solution.py:43
  418.1 4.5 reshape.246
  444.2 11.2 %collective-permute-done.2 = bf16[1,240,1024]{2,1,0:T(8,128)(2,1)S(1)} collective-permute-done((bf16[1,240,1024]{2,1,0:T(8,128)(2,1)S(1)}, bf16[1,240,1024]{2,1,0:T(8,128)(2,1)S(1)}, u32[]{:S(2)}, u32[]{:S(2)}) %collective-permute-start.2) | collective-permute-done | bytes 491552 | tf_op jit(solution)/shard_map/ppermute | solution.py:29
  456.1 32.0 %collective-permute-done.3 = bf16[1,240,1024]{2,1,0:T(8,128)(2,1)S(1)} collective-permute-done((bf16[1,240,1024]{2,1,0:T(8,128)(2,1)S(1)}, bf16[1,240,1024]{2,1,0:T(8,128)(2,1)S(1)}, u32[]{:S(2)}, u32[]{:S(2)}) %collective-permute-start.3) | collective-permute-done | bytes 491552 | tf_op jit(solution)/shard_map/ppermute | solution.py:29
  489.0 9.8 %collective-permute-done.4 = bf16[1,240,1024]{2,1,0:T(8,128)(2,1)S(1)} collective-permute-done((bf16[1,240,1024]{2,1,0:T(8,128)(2,1)S(1)}, bf16[1,240,1024]{2,1,0:T(8,128)(2,1)S(1)}, u32[]{:S(2)}, u32[]{:S(2)}) %collective-permute-start.4) | collective-permute-done | bytes 491552 | tf_op jit(solution)/shard_map/ppermute | solution.py:29
  499.7 10.8 %collective-permute-done.5 = bf16[1,240,1024]{2,1,0:T(8,128)(2,1)S(1)} collective-permute-done((bf16[1,240,1024]{2,1,0:T(8,128)(2,1)S(1)}, bf16[1,240,1024]{2,1,0:T(8,128)(2,1)S(1)}, u32[]{:S(2)}, u32[]{:S(2)}) %collective-permute-start.5) | collective-permute-done | bytes 491552 | tf_op jit(solution)/shard_map/ppermute | solution.py:29
  511.3 10.6 %collective-permute-done.6 = bf16[1,240,1024]{2,1,0:T(8,128)(2,1)S(1)} collective-permute-done((bf16[1,240,1024]{2,1,0:T(8,128)(2,1)S(1)}, bf16[1,240,1024]{2,1,0:T(8,128)(2,1)S(1)}, u32[]{:S(2)}, u32[]{:S(2)}) %collective-permute-start.6) | collective-permute-done | bytes 491552 | tf_op jit(solution)/shard_map/ppermute | solution.py:29
  522.7 4.8 gather_fusion
  527.5 9.7 %gather_fusion.1 = bf16[1536,1024]{1,0:T(8,128)(2,1)S(1)} fusion(bf16[1920,1024]{1,0:T(8,128)(2,1)} %bitcast.84, s32[2048]{0:T(1024)S(1)} %pad_clamp_fusion), kind=kCustom, calls=%fused_computation.2 | custom fusion | bytes 6297600 | tf_op jit(solution)/shard_map/gather | solution.py:82
  537.2 4.4 reshape.199
  541.6 7.9 %multiply_reduce_fusion = bf16[384,1024]{1,0:T(8,128)(2,1)} fusion(f32[384,4,1024]{2,1,0:T(4,128)} %reshape.199, f32[384,4]{1,0:T(8,128)S(1)} %copy.33), kind=kLoop, calls=%fused_computation.7 | loop fusion | flops 2752512 | bytes 7084032 | tf_op jit(solution)/shard_map/reduce_sum | solution.py:84
  (69 shorter events, 62.0 us)
Async XLA Ops:
  14.0 5.7 %copy-start.5 = (s32[384,4]{0,1:T(4,128)S(1)}, s32[384,4]{0,1:T(4,128)}, u32[]{:S(2)}) copy-start(s32[384,4]{0,1:T(4,128)} %param.8) | copy-start | bytes 18436
  14.0 51.3 %all-to-all-start = ((bf16[8,256,512]{2,1,0:T(8,128)(2,1)}), bf16[8,256,512]{2,1,0:T(8,128)(2,1)S(1)}, u32[]{:S(2)}, u32[]{:S(2)}) async-start(bf16[8,256,512]{2,1,0:T(8,128)(2,1)} %get-tuple-element.25), calls=%async_computation | async-start | bytes 4194304 | tf_op jit(solution)/shard_map/all_to_all | solution.py:39
  65.3 185.9 %copy-start = (bf16[8,256,512]{2,1,0:T(8,128)(2,1)}, bf16[8,256,512]{2,1,0:T(8,128)(2,1)S(1)}, u32[]{:S(2)}) copy-start(bf16[8,256,512]{2,1,0:T(8,128)(2,1)S(1)} %all-to-all-done) | copy-start | bytes 6291460
  244.0 52.8 %all-to-all-start.1 = ((bf16[8,256,512]{2,1,0:T(8,128)(2,1)}), bf16[8,256,512]{2,1,0:T(8,128)(2,1)}, u32[]{:S(2)}, u32[]{:S(2)}) async-start(bf16[8,256,512]{2,1,0:T(8,128)(2,1)} %get-tuple-element.24), calls=%async_computation.1 | async-start | bytes 4194304 | tf_op jit(solution)/shard_map/all_to_all | solution.py:40
  251.2 142.4 %all-gather.3.cloned.1.call-start = ((), (), s32[]{:S(2)}) async-start(), calls=%async_computation.5 | async-start | bytes 5898240 | tf_op jit(solution)/shard_map/all_gather | solution.py:72
  312.2 52.9 %all-to-all-start.2 = ((bf16[8,128,1024]{2,1,0:T(8,128)(2,1)}), bf16[8,128,1024]{2,1,0:T(8,128)(2,1)S(1)}, u32[]{:S(2)}, u32[]{:S(2)}) async-start(bf16[8,128,1024]{2,1,0:T(8,128)(2,1)} %convert_element_type.60), calls=%async_computation.2 | async-start | bytes 4194304 | tf_op jit(solution)/shard_map/all_to_all | solution.py:42
  388.6 29.4 %all-to-all-start.3 = ((bf16[2,2,262144]{2,1,0:T(2,128)(2,1)}), bf16[2,2,262144]{2,1,0:T(2,128)(2,1)}, u32[]{:S(2)}, u32[]{:S(2)}) async-start(bf16[2,2,262144]{2,1,0:T(2,128)(2,1)} %reshape.245), calls=%async_computation.3 | async-start | bytes 4194304 | tf_op jit(solution)/shard_map/all_to_all | solution.py:43
  393.6 3.9 copy-start.7
  399.8 5.3 copy-start.6
  401.5 35.8 %collective-permute-start = (bf16[1,240,1024]{2,1,0:T(8,128)(2,1)}, bf16[1,240,1024]{2,1,0:T(8,128)(2,1)}, u32[]{:S(2)}, u32[]{:S(2)}) collective-permute-start(bf16[1,240,1024]{2,1,0:T(8,128)(2,1)} %get-tuple-element.22), channel_id=1, source_target_pairs={{0,2},{2,0},{4,6},{6,4},{8,10},{10,8},{12,14},{14,12},{1,3},{3,1},... | collective-permute-start | bytes 1474568 | tf_op jit(solution)/shard_map/ppermute | solution.py:29
  401.9 38.3 %collective-permute-start.1 = (bf16[1,240,1024]{2,1,0:T(8,128)(2,1)}, bf16[1,240,1024]{2,1,0:T(8,128)(2,1)}, u32[]{:S(2)}, u32[]{:S(2)}) collective-permute-start(bf16[1,240,1024]{2,1,0:T(8,128)(2,1)} %get-tuple-element.21), channel_id=1, source_target_pairs={{0,4},{2,6},{4,0},{6,2},{8,12},{10,14},{12,8},{14,10},{1,5},{3,7},... | collective-permute-start | bytes 1474568 | tf_op jit(solution)/shard_map/ppermute | solution.py:29
  428.1 4.0 copy-start.4
  428.1 7.9 %copy-start.3 = (bf16[1,240,1024]{2,1,0:T(8,128)(2,1)S(1)}, bf16[1,240,1024]{2,1,0:T(8,128)(2,1)}, u32[]{:S(2)}) copy-start(bf16[1,240,1024]{2,1,0:T(8,128)(2,1)} %get-tuple-element.19) | copy-start | bytes 1474564
  428.1 7.9 %copy-start.2 = (bf16[1,240,1024]{2,1,0:T(8,128)(2,1)S(1)}, bf16[1,240,1024]{2,1,0:T(8,128)(2,1)}, u32[]{:S(2)}) copy-start(bf16[1,240,1024]{2,1,0:T(8,128)(2,1)} %get-tuple-element.18) | copy-start | bytes 1474564
  432.2 23.1 %collective-permute-start.2 = (bf16[1,240,1024]{2,1,0:T(8,128)(2,1)S(1)}, bf16[1,240,1024]{2,1,0:T(8,128)(2,1)S(1)}, u32[]{:S(2)}, u32[]{:S(2)}) collective-permute-start(bf16[1,240,1024]{2,1,0:T(8,128)(2,1)S(1)} %copy-done.4), channel_id=1, source_target_pairs={{0,6},{2,4},{4,2},{6,0},{8,14},{10,12},{12,10},{14,8},{1,7},{3,5},... | collective-permute-start | bytes 1474568 | tf_op jit(solution)/shard_map/ppermute | solution.py:29
  436.0 52.1 %collective-permute-start.3 = (bf16[1,240,1024]{2,1,0:T(8,128)(2,1)S(1)}, bf16[1,240,1024]{2,1,0:T(8,128)(2,1)S(1)}, u32[]{:S(2)}, u32[]{:S(2)}) collective-permute-start(bf16[1,240,1024]{2,1,0:T(8,128)(2,1)S(1)} %copy-done.3), channel_id=1, source_target_pairs={{0,8},{2,10},{4,12},{6,14},{8,0},{10,2},{12,4},{14,6},{1,9},{3,11}... | collective-permute-start | bytes 1474568 | tf_op jit(solution)/shard_map/ppermute | solution.py:29
  436.1 62.8 %collective-permute-start.4 = (bf16[1,240,1024]{2,1,0:T(8,128)(2,1)S(1)}, bf16[1,240,1024]{2,1,0:T(8,128)(2,1)S(1)}, u32[]{:S(2)}, u32[]{:S(2)}) collective-permute-start(bf16[1,240,1024]{2,1,0:T(8,128)(2,1)S(1)} %copy-done.2), channel_id=1, source_target_pairs={{0,10},{2,8},{4,14},{6,12},{8,2},{10,0},{12,6},{14,4},{1,11},{3,9}... | collective-permute-start | bytes 1474568 | tf_op jit(solution)/shard_map/ppermute | solution.py:29
  437.3 73.2 %collective-permute-start.5 = (bf16[1,240,1024]{2,1,0:T(8,128)(2,1)S(1)}, bf16[1,240,1024]{2,1,0:T(8,128)(2,1)S(1)}, u32[]{:S(2)}, u32[]{:S(2)}) collective-permute-start(bf16[1,240,1024]{2,1,0:T(8,128)(2,1)S(1)} %get-tuple-element.17), channel_id=1, source_target_pairs={{0,12},{2,14},{4,8},{6,10},{8,4},{10,6},{12,0},{14,2},{1,13},{3,15... | collective-permute-start | bytes 1474568 | tf_op jit(solution)/shard_map/ppermute | solution.py:29
  440.2 81.7 %collective-permute-start.6 = (bf16[1,240,1024]{2,1,0:T(8,128)(2,1)S(1)}, bf16[1,240,1024]{2,1,0:T(8,128)(2,1)S(1)}, u32[]{:S(2)}, u32[]{:S(2)}) collective-permute-start(bf16[1,240,1024]{2,1,0:T(8,128)(2,1)S(1)} %get-tuple-element.16), channel_id=1, source_target_pairs={{0,14},{2,12},{4,10},{6,8},{8,6},{10,4},{12,2},{14,0},{1,15},{3,13... | collective-permute-start | bytes 1474568 | tf_op jit(solution)/shard_map/ppermute | solution.py:29
  541.6 7.9 %copy-start.1 = (bf16[8,256,512]{2,1,0:T(8,128)(2,1)S(1)}, bf16[8,256,512]{2,1,0:T(8,128)(2,1)}, u32[]{:S(2)}) copy-start(bf16[8,256,512]{2,1,0:T(8,128)(2,1)} %copy-done) | copy-start | bytes 6291460
Sparse Core Ops, SparseCore 0:
  308.5 55.3 all-gather.2
